TPU v7x, 32 devices: a whole 2x2x4 slice. The times are simulated.
32 devices in a mesh: sp: 4 (over y, x), dp: 8 (over z, core).
Axes of the slice: x: 2, y: 2, z: 4, core: 2. Of those that a mesh axis runs over, the one named last changes fastest.
Arguments:
- tokens: bfloat16 [8, 512, 2048], P('dp', 'sp'), may hold values from -6 to 6
- query_weight: bfloat16 [2048, 1024], P('dp'), may hold values from -0.125 to 0.125
- key_weight: bfloat16 [2048, 1024], P('dp'), may hold values from -0.125 to 0.125
- value_weight: bfloat16 [2048, 2048], P('dp'), may hold values from -0.125 to 0.125
- output_weight: bfloat16 [2048, 2048], P('dp'), may hold values from -0.125 to 0.125
- log_decay: float32 [2, 16], P(None, 'sp'), may hold values from -0.04 to 0, as said below
Outputs:
- mixed: bfloat16 [8, 512, 2048], P('dp', 'sp')
Inputs may be any that keep to these rules, and one draw needn't show every extreme that they name: `log_decay`: every entry is negative: the logarithm of a head's decay per position.
All inputs are finite; a program needn't handle non-finite values.
Results may differ from a plain program's by a relative error of at most 0.012.
Values may be sent and summed in bfloat16 or wider, within the bound.
A program may use at most 128 MiB of HBM per device.

v0:
```python
import jax
import jax.numpy as jnp
from jax import lax
from jax.sharding import PartitionSpec as P

HEADS = 16
DK = 64
DV = 128
BLOCK = 512
exact_precision = lax.Precision.HIGHEST


def rotate(values_part, positions):
    half_dim = values_part.shape[-1] // 2
    frequency = 10000.0 ** (-jnp.arange(half_dim, dtype=jnp.float32) / half_dim)
    angles = positions[:, None] * frequency[None, :]
    cosine = jnp.cos(angles)[:, None, :]
    sine_part = jnp.sin(angles)[:, None, :]
    first = values_part[..., :half_dim]
    second = values_part[..., half_dim:]
    return jnp.concatenate(
        [first * cosine - second * sine_part, first * sine_part + second * cosine], axis=-1
    )


def retain(query, key_rows, value_rows, log_rate):
    length, heads, key_dim = query.shape
    value_dim = value_rows.shape[-1]
    count = length // BLOCK
    offsets = jnp.arange(BLOCK, dtype=jnp.float32)
    distance = offsets[:, None] - offsets[None, :]
    decay_inner = jnp.where(
        distance[None] >= 0.0,
        jnp.exp(log_rate[:, None, None] * jnp.maximum(distance, 0.0)[None]),
        0.0,
    )
    decay_query = jnp.exp((offsets[:, None] + 1.0) * log_rate[None, :])[:, :, None]
    decay_key = jnp.exp((BLOCK - 1.0 - offsets)[:, None] * log_rate[None, :])[:, :, None]
    decay_block = jnp.exp(BLOCK * log_rate)[:, None, None]

    def blocks(array):
        return array.reshape(count, BLOCK, heads, array.shape[-1])

    def advance(state, inputs):
        query_block, key_block, value_block = inputs
        inner = (
            jnp.einsum("ihd,jhd->hij", query_block, key_block, preferred_element_type=jnp.float32)
            * decay_inner
        )
        result = jnp.einsum(
            "hij,jhv->ihv",
            inner.astype(jnp.bfloat16),
            value_block,
            preferred_element_type=jnp.float32,
        )
        query_wide = query_block.astype(jnp.float32) * decay_query
        result = result + jnp.einsum("ihd,hdv->ihv", query_wide, state, precision=exact_precision)
        key_wide = key_block.astype(jnp.float32) * decay_key
        state = state * decay_block + jnp.einsum(
            "jhd,jhv->hdv", key_wide, value_block.astype(jnp.float32), precision=exact_precision
        )
        return (state, result)

    initial = jnp.zeros((heads, key_dim, value_dim), jnp.float32)
    final_state, outputs = lax.scan(
        advance, initial, (blocks(query), blocks(key_rows), blocks(value_rows))
    )
    return outputs.reshape(length, heads, value_dim)


def mechanism(stacked, log_decay):
    length = stacked.shape[0]
    widened = stacked[..., : 2 * DK].astype(jnp.float32)
    positions = jnp.arange(length, dtype=jnp.float32)
    query = rotate(widened[..., :DK], positions).astype(jnp.bfloat16)
    key_rows = rotate(widened[..., DK : 2 * DK], positions).astype(jnp.bfloat16)
    value_rows = stacked[..., 2 * DK :]
    forward = retain(query, key_rows, value_rows, log_decay[0])
    backward = retain(
        jnp.flip(query, 0), jnp.flip(key_rows, 0), jnp.flip(value_rows, 0), log_decay[1]
    )
    combined = forward + jnp.flip(backward, 0)
    average = jnp.mean(combined, axis=-1, keepdims=True)
    centred = combined - average
    variance = jnp.mean(centred * centred, axis=-1, keepdims=True)
    return (centred * lax.rsqrt(variance + 1e-06)).astype(jnp.bfloat16)


def shards(tokens, query_weight, key_weight, value_weight, output_weight, log_decay):
    rows = tokens[0]
    row_count = rows.shape[0]
    local_heads = log_decay.shape[1]
    first_head = lax.axis_index("sp") * local_heads
    own_slices = jnp.concatenate(
        [
            lax.dynamic_slice_in_dim(query_weight, first_head * DK, local_heads * DK, 1),
            lax.dynamic_slice_in_dim(key_weight, first_head * DK, local_heads * DK, 1),
            lax.dynamic_slice_in_dim(value_weight, first_head * DV, local_heads * DV, 1),
        ],
        axis=1,
    )
    own_whole = lax.all_gather(own_slices, "dp", axis=0, tiled=True)
    piece = lax.all_gather(rows, "sp", axis=0, tiled=True)
    count = piece.shape[0]
    product = jnp.dot(piece, own_whole, preferred_element_type=jnp.float32).astype(jnp.bfloat16)
    query_part = product[:, : local_heads * DK].reshape(count, local_heads, DK)
    key_part = product[:, local_heads * DK : 2 * local_heads * DK].reshape(count, local_heads, DK)
    value_part = product[:, 2 * local_heads * DK :].reshape(count, local_heads, DV)
    gathered = jnp.concatenate([query_part, key_part, value_part], axis=2)
    normed = mechanism(gathered, log_decay)
    by_token = lax.all_to_all(normed, "sp", split_axis=0, concat_axis=1, tiled=True).reshape(
        row_count, HEADS * DV
    )
    mixed = jnp.dot(
        by_token,
        lax.all_gather(output_weight, "dp", axis=0, tiled=True),
        preferred_element_type=jnp.float32,
    )
    return mixed.astype(jnp.bfloat16)[None]


def solution(mesh):
    placed = (
        P("dp", "sp", None),
        P("dp", None),
        P("dp", None),
        P("dp", None),
        P("dp", None),
        P(None, "sp"),
    )
    return jax.shard_map(
        shards, mesh=mesh, in_specs=placed, out_specs=P("dp", "sp", None), check_vma=False
    )
```

profile of v0, /device:TPU:0, one launch (start us, length us, event | category | flops | bytes accessed | tf_op | source)
XLA Modules:
  0.0 190.1 jit_solution(7368320106620068643)
XLA Ops:
  6.5 0.7 all-gather.9.cloned.1.call-update
  7.3 0.4 copy-done
  7.8 1.0 constant_dynamic-slice_fusion.1
  8.8 0.9 pad_maximum_fusion
  9.7 0.7 all-gather.7.cloned.1.call-update
  10.4 1.0 fusion.15
  11.4 0.2 fusion.14
  11.7 0.3 fusion.25
  12.0 35.1 %all-gather.9.cloned.1.call-done = bf16[1,512,2048]{2,1,0:T(8,128)(2,1)} async-done(((bf16[1,128,2048]{2,1,0:T(8,128)(2,1)}), bf16[1,512,2048]{2,1,0:T(8,128)(2,1)}) %all-gather.9.cloned.1.call-update) | async-done | bytes 2097168 | tf_op jit(solution)/shard_map/all_gather | solution.py:103
  47.1 48.5 %all-gather.5.cloned.1.call-done = bf16[2048,1024]{1,0:T(8,128)(2,1)} async-done(((bf16[256,1024]{1,0:T(8,128)(2,1)}), bf16[2048,1024]{1,0:T(8,128)(2,1)}) %all-gather.5.cloned.1.call-update) | async-done | bytes 4194320 | tf_op jit(solution)/shard_map/all_gather | solution.py:102
  95.6 5.2 %fusion.8 = bf16[512,1024]{0,1:T(8,128)(2,1)S(1)} fusion(bf16[2048,1024]{1,0:T(8,128)(2,1)} %all-gather.5.cloned.1.call-done, bf16[1,512,2048]{2,1,0:T(8,128)(2,1)} %all-gather.9.cloned.1.call-done), kind=kOutput, calls=%fused_computation.9 | convolution fusion | flops 2148007936 | bytes 7340032 | tf_op jit(solution)/shard_map/dot_general | solution.py:105
  101.3 1.6 rev.17
  103.0 0.5 rev.16
  103.5 5.7 %rev.15 = bf16[512,4,128]{0,2,1:T(8,128)(2,1)} reverse(bf16[512,4,128]{0,2,1:T(8,128)(2,1)S(1)} %bitcast.36), dimensions={0} | reverse | bytes 1048576 | tf_op jit(solution)/shard_map/jit(_flip)/rev | solution.py:80
  109.2 4.2 %fusion.4 = f32[4,128,512]{2,1,0:T(8,128)} fusion(bf16[512,4,128]{0,2,1:T(8,128)(2,1)} %rev.15, bf16[512,4,64]{0,2,1:T(8,128)(2,1)S(1)} %rev.16, bf16[512,4,64]{0,2,1:T(8,128)(2,1)} %rev.17, f32[4]{0:T(128)} %copy-done.5, f32[512,512]{1,0:T(8,128)S(1)} %fusion.14, pred[512,512]{1,0:T(8,128)(4,1)} %fusion.15), kind=kOutput, calls=%fused_computation.7 | convolution fusion | flops 406847488 | bytes 3407888 | tf_op jit(solution)/shard_map/while/body/eval_jaxpr/hij,jhv->ihv/dot_general | solution.py:50
  113.4 2.2 %fusion.11 = f32[512,4,128]{0,2,1:T(8,128)S(1)} fusion(f32[4,128,512]{2,1,0:T(8,128)} %fusion.4, bf16[512,4,64]{0,2,1:T(8,128)(2,1)S(1)} %rev.16, f32[512,4]{0,1:T(4,128)S(1)} %get-tuple-element.60), kind=kOutput, calls=%fused_computation.11 | convolution fusion | flops 201850880 | bytes 2367488 | tf_op jit(solution)/shard_map/while/body/eval_jaxpr/ihd,hdv->ihv/dot_general | solution.py:57
  115.6 1.5 rev.18
  117.0 3.4 %fusion.3 = f32[4,128,512]{2,1,0:T(8,128)S(1)} fusion(bf16[512,4,128]{0,2,1:T(8,128)(2,1)} %bitcast.37, f32[512,512]{1,0:T(8,128)} %copy-done.2, f32[4]{0:T(128)} %copy-done.4, pred[512,512]{1,0:T(8,128)(4,1)} %fusion.15, bf16[512,4,32]{0,2,1:T(8,128)(2,1)} %copy-done.3, bf16[512,4,32]{0,2,1:T(8,128)(2,1)S(1)} %get-tuple-element.43, ...), kind=kOutput, calls=%fused_computation.6 | convolution fusion | flops 407896064 | bytes 3407888 | tf_op jit(solution)/shard_map/while/body/eval_jaxpr/hij,jhv->ihv/dot_general | solution.py:50
  120.5 1.0 fusion.31
  121.8 0.3 copy.9
  122.1 12.3 %all_to_all.15 = bf16[512,4,128]{2,1,0:T(4,128)(2,1)S(1)} all-to-all(bf16[512,4,128]{2,1,0:T(4,128)(2,1)S(1)} %copy.9), channel_id=1, replica_groups=mesh['sp'=4,'dp'=8] {'sp'}, dimensions={0} | all-to-all | bytes 1048576 | tf_op jit(solution)/shard_map/all_to_all | solution.py:111
  134.6 0.3 copy.11
  134.8 43.3 %all-gather.7.cloned.1.call-done = bf16[2048,2048]{1,0:T(8,128)(2,1)} async-done(((bf16[256,2048]{1,0:T(8,128)(2,1)}), bf16[2048,2048]{1,0:T(8,128)(2,1)}) %all-gather.7.cloned.1.call-update) | async-done | bytes 8388624 | tf_op jit(solution)/shard_map/all_gather | solution.py:116
  178.1 5.5 %fusion = bf16[1,128,2048]{2,1,0:T(8,128)(2,1)} fusion(bf16[128,2048]{0,1:T(8,128)(2,1)S(1)} %bitcast.35, bf16[2048,2048]{1,0:T(8,128)(2,1)} %all-gather.7.cloned.1.call-done), kind=kOutput, calls=%fused_computation.3 | convolution fusion | flops 1074003968 | bytes 9437184 | tf_op jit(solution)/shard_map/dot_general | solution.py:114
  (33 shorter events, 1.0 us)
Async XLA Ops:
  6.5 1.2 copy-start
  6.5 5.0 %copy-start.6 = (f32[2,4]{1,0:T(2,128)S(1)}, f32[2,4]{1,0:T(2,128)}, u32[]{:S(2)}) copy-start(f32[2,4]{1,0:T(2,128)} %param.11) | copy-start | bytes 100
  6.5 40.6 %all-gather.9.cloned.1.call-start = ((), (), s32[]{:S(2)}) async-start(), calls=%async_computation.3 | async-start | bytes 2621440 | tf_op jit(solution)/shard_map/all_gather | solution.py:103
  7.3 88.3 %all-gather.5.cloned.1.call-start = ((), (), s32[]{:S(2)}) async-start(), calls=%async_computation.1 | async-start | bytes 4718592 | tf_op jit(solution)/shard_map/all_gather | solution.py:102
  9.7 168.5 %all-gather.7.cloned.1.call-start = ((), (), s32[]{:S(2)}) async-start(), calls=%async_computation.2 | async-start | bytes 9437184 | tf_op jit(solution)/shard_map/all_gather | solution.py:116
  11.6 97.6 %copy-start.2 = (f32[512,512]{1,0:T(8,128)}, f32[512,512]{1,0:T(8,128)S(1)}, u32[]{:S(2)}) copy-start(f32[512,512]{1,0:T(8,128)S(1)} %fusion.14) | copy-start | bytes 3145732
  11.6 89.3 %copy-start.4 = (f32[4]{0:T(128)}, f32[4]{0:T(128)S(1)}, u32[]{:S(2)}) copy-start(f32[4]{0:T(128)S(1)} %get-tuple-element.61) | copy-start | bytes 52
  11.6 89.3 %copy-start.5 = (f32[4]{0:T(128)}, f32[4]{0:T(128)S(1)}, u32[]{:S(2)}) copy-start(f32[4]{0:T(128)S(1)} %get-tuple-element.62) | copy-start | bytes 52
  100.9 12.4 %copy-start.1 = (bf16[512,512]{0,1:T(8,128)(2,1)}, bf16[512,512]{0,1:T(8,128)(2,1)S(1)}, u32[]{:S(2)}) copy-start(bf16[512,512]{0,1:T(8,128)(2,1)S(1)} %slice.42) | copy-start | bytes 1572868
  101.3 1.7 copy-start.3
Sparse Core Ops, SparseCore 0:
  9.2 37.8 all-gather.8
  48.7 46.8 all-gather.4
  97.2 80.8 all-gather.6
where the time goes:
time: 190 us
  waiting for transfers between devices  128 us (67%)
  matrix products  21.5 us (11%)
  between operations  13.3 us (7%)
  blocking collectives  12.3 us (6%)
  local copies, waits for them, and re-layouts  11.6 us (6%)
  other arithmetic  3.01 us (2%)
    all_gather x1, waiting for transfers between devices, shards(): own_whole = lax.all_gather(own_slices, 'dp', axis=0, tiled=True)  48.5 us
    all_gather x1, waiting for transfers between devices, shards(): lax.all_gather(output_weight, 'dp', axis=0, tiled=True)  43.3 us
    all_gather x1, waiting for transfers between devices, shards(): piece = lax.all_gather(rows, 'sp', axis=0, tiled=True)  35.1 us
    all_to_all x1, blocking collectives, shards(): lax.all_to_all(normed, 'sp', split_axis=0, concat_axis=1, tiled=True)  12.3 us
    dot_general x2, matrix products, advance(): jnp.einsum('hij,jhv->ihv', inner.astype(jnp.bfloat16), value_block, prefe...  7.56 us
    rev x1, local copies, waits for them, and re-layouts, mechanism(): jnp.flip(value_rows, 0)  5.71 us
    dot_general x1, matrix products, shards(): jnp.dot(by_token, lax.all_gather(output_weight, 'dp', axis=0, tiled=True)...  5.46 us
    dot_general x1, matrix products, shards(): jnp.dot(piece, own_whole, preferred_element_type=jnp.float32)  5.25 us
  transfers between devices with their start and end apart: 3, of which 3 were waited for; matrix products, arithmetic and copies ran while one was open for 16% of the time, Pallas kernels for 0%

commit v1 on v0

--- a/solution.py
+++ b/solution.py
@@ -100,7 +100,17 @@
         axis=1,
     )
     own_whole = lax.all_gather(own_slices, "dp", axis=0, tiled=True)
-    piece = lax.all_gather(rows, "sp", axis=0, tiled=True)
+    axis_len = lax.axis_size("sp")
+    odd = sorted(((i0, (i0 + 1) % axis_len) for i0 in range(axis_len)))
+    carry_out = rows
+    pages = [carry_out]
+    for idx in tuple(range(1, axis_len)):
+        carry_out = lax.ppermute(carry_out, "sp", odd)
+        pages.insert(0, carry_out)
+    built = jnp.concatenate(pages, axis=0)
+    state_now = lax.axis_index("sp")
+    inter = state_now + 1
+    piece = jnp.roll(built, inter * rows.shape[0], 0)
     count = piece.shape[0]
     product = jnp.dot(piece, own_whole, preferred_element_type=jnp.float32).astype(jnp.bfloat16)
     query_part = product[:, : local_heads * DK].reshape(count, local_heads, DK)

time: 190 us -> 155 us (0.82)
  waiting for transfers between devices: 128 us -> 77.3 us
  local copies, waits for them, and re-layouts: 11.6 us -> 20.4 us
  starting transfers between devices: 0.08 us -> 3.85 us
  other arithmetic: 3.01 us -> 6.75 us
    all_gather x1, waiting for transfers between devices: 48.5 us -> 0.01 us  [shards(): own_whole = lax.all_gather(own_slices, 'dp', axis=0, tiled=True)]
    ppermute x0 -> x3, waiting for transfers between devices: none -> 36.5 us  [shards(): carry_out = lax.ppermute(carry_out, 'sp', odd)]
    all_gather x1 -> x0, waiting for transfers between devices: 35.1 us -> none  [shards(): piece = lax.all_gather(rows, 'sp', axis=0, tiled=True)]
    unnamed x14 -> x23, local copies, waits for them, and re-layouts: 0.47 us -> 7.23 us
    ppermute x0 -> x3, starting transfers between devices: none -> 3.8 us  [shards(): carry_out = lax.ppermute(carry_out, 'sp', odd)]
    all_gather x1, waiting for transfers between devices: 43.3 us -> 40.1 us  [shards(): lax.all_gather(output_weight, 'dp', axis=0, tiled=True)]
  transfers between devices with their start and end apart: 3 -> 5, of which waited for: 3 -> 4; matrix products, arithmetic and copies ran while one was open for 16% -> 26% of each run, Pallas kernels for 0% -> 0%
where the time goes in v1:
time: 155 us; the launch traced here: 154 us
  waiting for transfers between devices  77.3 us (50%)
  matrix products  21.4 us (14%)
  local copies, waits for them, and re-layouts  20.4 us (13%)
  between operations  13.6 us (9%)
  blocking collectives  10.9 us (7%)
  other arithmetic  6.75 us (4%)
  starting transfers between devices  3.85 us (2%)
    all_gather x1, waiting for transfers between devices, shards(): lax.all_gather(output_weight, 'dp', axis=0, tiled=True)  40.1 us
    ppermute x3, waiting for transfers between devices, shards(): carry_out = lax.ppermute(carry_out, 'sp', odd)  36.5 us
    all_to_all x1, blocking collectives, shards(): lax.all_to_all(normed, 'sp', split_axis=0, concat_axis=1, tiled=True)  10.9 us
    dot_general x2, matrix products, advance(): jnp.einsum('hij,jhv->ihv', inner.astype(jnp.bfloat16), value_block, prefe...  7.6 us
    unnamed x23, local copies, waits for them, and re-layouts  7.23 us
    rev x1, local copies, waits for them, and re-layouts, mechanism(): jnp.flip(value_rows, 0)  5.71 us
    dot_general x1, matrix products, shards(): jnp.dot(by_token, lax.all_gather(output_weight, 'dp', axis=0, tiled=True)...  5.46 us
    dot_general x1, matrix products, shards(): jnp.dot(piece, own_whole, preferred_element_type=jnp.float32)  5.15 us
  transfers between devices with their start and end apart: 5, of which 4 were waited for; matrix products, arithmetic and copies ran while one was open for 26% of the time, Pallas kernels for 0%

profile of v1, /device:TPU:0, one launch (start us, length us, event | category | flops | bytes accessed | tf_op | source)
XLA Modules:
  0.0 154.2 jit_solution(15698099767894030324)
XLA Ops:
  6.6 1.2 copy-done
  7.8 1.0 constant_dynamic-slice_fusion.1
  10.4 3.0 %collective-permute-start = (bf16[128,2048]{1,0:T(8,128)(2,1)}, bf16[128,2048]{1,0:T(8,128)(2,1)S(1)}, u32[]{:S(2)}, u32[]{:S(2)}) collective-permute-start(bf16[128,2048]{1,0:T(8,128)(2,1)} %bitcast.30), channel_id=1, source_target_pairs={{0,8},{8,16},{16,24},{24,0},{1,9},{9,17},{17,25},{25,1},{2,10},{10... | collective-permute-start | bytes 1572872 | tf_op jit(solution)/shard_map/ppermute | solution.py:108
  13.5 13.1 %collective-permute-done = bf16[128,2048]{1,0:T(8,128)(2,1)S(1)} collective-permute-done((bf16[128,2048]{1,0:T(8,128)(2,1)}, bf16[128,2048]{1,0:T(8,128)(2,1)S(1)}, u32[]{:S(2)}, u32[]{:S(2)}) %collective-permute-start) | collective-permute-done | bytes 524320 | tf_op jit(solution)/shard_map/ppermute | solution.py:108
  27.3 1.0 fusion.12
  28.3 1.2 fusion.11
  29.5 11.2 %collective-permute-done.1 = bf16[128,2048]{1,0:T(8,128)(2,1)S(1)} collective-permute-done((bf16[128,2048]{1,0:T(8,128)(2,1)S(1)}, bf16[128,2048]{1,0:T(8,128)(2,1)S(1)}, u32[]{:S(2)}, u32[]{:S(2)}) %collective-permute-start.1) | collective-permute-done | bytes 524320 | tf_op jit(solution)/shard_map/ppermute | solution.py:108
  40.7 1.0 fusion.22
  41.7 12.3 %collective-permute-done.2 = bf16[128,2048]{1,0:T(8,128)(2,1)S(1)} collective-permute-done((bf16[128,2048]{1,0:T(8,128)(2,1)S(1)}, bf16[128,2048]{1,0:T(8,128)(2,1)S(1)}, u32[]{:S(2)}, u32[]{:S(2)}) %collective-permute-start.2) | collective-permute-done | bytes 524320 | tf_op jit(solution)/shard_map/ppermute | solution.py:108
  54.0 0.9 constant_dynamic-update-slice_fusion.7
  58.2 0.9 constant_dynamic-update-slice_fusion.2
  60.8 5.2 %fusion.5 = bf16[512,1024]{1,0:T(8,128)(2,1)S(1)} fusion(bf16[2048,1024]{1,0:T(8,128)(2,1)} %all-gather.3.cloned.1.call-done, bf16[1024,2048]{1,0:T(8,128)(2,1)} %constant_dynamic-update-slice_fusion, s32[]{:T(128)S(6)} %select_n.28), kind=kOutput, calls=%fused_computation.8 | convolution fusion | flops 2148007936 | bytes 7340036 | tf_op jit(solution)/shard_map/dot_general | solution.py:115
  67.3 1.3 maximum_convert_fusion
  68.6 1.1 subtract_convert_fusion
  69.7 1.6 %rev.17 = bf16[512,4,64]{0,2,1:T(8,128)(2,1)} reverse(bf16[512,4,64]{0,2,1:T(8,128)(2,1)S(1)} %pad_maximum_fusion.2), dimensions={0} | reverse | bytes 524288 | tf_op jit(solution)/shard_map/jit(_flip)/rev | solution.py:80
  71.9 5.7 %rev.15 = bf16[512,4,128]{0,2,1:T(8,128)(2,1)} reverse(bf16[512,4,128]{0,2,1:T(8,128)(2,1)S(1)} %bitcast.31), dimensions={0} | reverse | bytes 1048576 | tf_op jit(solution)/shard_map/jit(_flip)/rev | solution.py:80
  77.6 4.2 %fusion.4 = f32[4,128,512]{2,1,0:T(8,128)} fusion(bf16[512,4,128]{0,2,1:T(8,128)(2,1)} %rev.15, bf16[512,4,64]{0,2,1:T(8,128)(2,1)S(1)} %rev.16, bf16[512,4,64]{0,2,1:T(8,128)(2,1)} %rev.17, f32[4]{0:T(128)} %copy-done.6, f32[512,512]{1,0:T(8,128)S(1)} %copy-done.3, pred[512,512]{1,0:T(8,128)(4,1)} %fusion.12), kind=kOutput, calls=%fused_computation.7 | convolution fusion | flops 406847488 | bytes 3407888 | tf_op jit(solution)/shard_map/while/body/eval_jaxpr/hij,jhv->ihv/dot_general | solution.py:50
  81.8 2.2 %fusion.8 = f32[512,4,128]{0,2,1:T(8,128)S(1)} fusion(f32[4,128,512]{2,1,0:T(8,128)} %fusion.4, bf16[512,4,64]{0,2,1:T(8,128)(2,1)S(1)} %rev.16, f32[512,4]{0,1:T(4,128)S(1)} %get-tuple-element.60), kind=kOutput, calls=%fused_computation.10 | convolution fusion | flops 201850880 | bytes 2367488 | tf_op jit(solution)/shard_map/while/body/eval_jaxpr/ihd,hdv->ihv/dot_general | solution.py:57
  84.0 1.5 rev.18
  85.5 3.4 %fusion.3 = f32[4,128,512]{2,1,0:T(8,128)S(1)} fusion(bf16[512,4,128]{0,2,1:T(8,128)(2,1)} %bitcast.32, f32[512,512]{1,0:T(8,128)} %fusion.11, f32[4]{0:T(128)} %copy-done.5, pred[512,512]{1,0:T(8,128)(4,1)} %fusion.12, bf16[512,4,32]{0,2,1:T(8,128)(2,1)} %copy-done.4, bf16[512,4,32]{0,2,1:T(8,128)(2,1)S(1)} %get-tuple-element.43, ...), kind=kOutput, calls=%fused_computation.6 | convolution fusion | flops 407896064 | bytes 3407888 | tf_op jit(solution)/shard_map/while/body/eval_jaxpr/hij,jhv->ihv/dot_general | solution.py:50
  88.9 1.0 fusion.29
  90.6 10.9 %all_to_all.15 = bf16[512,4,128]{2,1,0:T(4,128)(2,1)S(1)} all-to-all(bf16[512,4,128]{2,1,0:T(4,128)(2,1)S(1)} %copy.25), channel_id=1, replica_groups=mesh['sp'=4,'dp'=8] {'sp'}, dimensions={0} | all-to-all | bytes 1048576 | tf_op jit(solution)/shard_map/all_to_all | solution.py:121
  101.8 40.1 %all-gather.5.cloned.1.call-done = bf16[2048,2048]{1,0:T(8,128)(2,1)} async-done(((bf16[256,2048]{1,0:T(8,128)(2,1)}), bf16[2048,2048]{1,0:T(8,128)(2,1)}) %all-gather.5.cloned.1.call-update) | async-done | bytes 8388624 | tf_op jit(solution)/shard_map/all_gather | solution.py:126
  141.9 5.5 %fusion = bf16[1,128,2048]{2,1,0:T(8,128)(2,1)} fusion(bf16[128,2048]{0,1:T(8,128)(2,1)S(1)} %bitcast.29, bf16[2048,2048]{1,0:T(8,128)(2,1)} %all-gather.5.cloned.1.call-done), kind=kOutput, calls=%fused_computation.3 | convolution fusion | flops 1074003968 | bytes 9437184 | tf_op jit(solution)/shard_map/dot_general | solution.py:124
  (49 shorter events, 10.4 us)
Async XLA Ops:
  6.5 1.2 copy-start
  6.5 50.0 %copy-start.1 = (bf16[1,128,2048]{2,1,0:T(8,128)(2,1)S(1)}, bf16[1,128,2048]{2,1,0:T(8,128)(2,1)}, u32[]{:S(2)}) copy-start(bf16[1,128,2048]{2,1,0:T(8,128)(2,1)} %param.6) | copy-start | bytes 1572868
  6.5 22.9 %copy-start.7 = (f32[2,4]{1,0:T(2,128)S(1)}, f32[2,4]{1,0:T(2,128)}, u32[]{:S(2)}) copy-start(f32[2,4]{1,0:T(2,128)} %param.11) | copy-start | bytes 100
  6.5 54.3 %all-gather.3.cloned.1.call-start = ((), (), s32[]{:S(2)}) async-start(), calls=%async_computation.1 | async-start | bytes 4718592 | tf_op jit(solution)/shard_map/all_gather | solution.py:102
  9.7 132.2 %all-gather.5.cloned.1.call-start = ((), (), s32[]{:S(2)}) async-start(), calls=%async_computation.2 | async-start | bytes 9437184 | tf_op jit(solution)/shard_map/all_gather | solution.py:126
  10.4 16.1 %collective-permute-start = (bf16[128,2048]{1,0:T(8,128)(2,1)}, bf16[128,2048]{1,0:T(8,128)(2,1)S(1)}, u32[]{:S(2)}, u32[]{:S(2)}) collective-permute-start(bf16[128,2048]{1,0:T(8,128)(2,1)} %bitcast.30), channel_id=1, source_target_pairs={{0,8},{8,16},{16,24},{24,0},{1,9},{9,17},{17,25},{25,1},{2,10},{10... | collective-permute-start | bytes 1572872 | tf_op jit(solution)/shard_map/ppermute | solution.py:108
  26.5 14.1 %collective-permute-start.1 = (bf16[128,2048]{1,0:T(8,128)(2,1)S(1)}, bf16[128,2048]{1,0:T(8,128)(2,1)S(1)}, u32[]{:S(2)}, u32[]{:S(2)}) collective-permute-start(bf16[128,2048]{1,0:T(8,128)(2,1)S(1)} %collective-permute-done), channel_id=1, source_target_pairs={{0,8},{8,16},{16,24},{24,0},{1,9},{9,17},{17,25},{25,1},{2,10},{10... | collective-permute-start | bytes 1572872 | tf_op jit(solution)/shard_map/ppermute | solution.py:108
  29.5 31.3 %copy-start.5 = (f32[4]{0:T(128)}, f32[4]{0:T(128)S(1)}, u32[]{:S(2)}) copy-start(f32[4]{0:T(128)S(1)} %get-tuple-element.61) | copy-start | bytes 52
  29.5 31.3 %copy-start.6 = (f32[4]{0:T(128)}, f32[4]{0:T(128)S(1)}, u32[]{:S(2)}) copy-start(f32[4]{0:T(128)S(1)} %get-tuple-element.62) | copy-start | bytes 52
  40.6 13.3 %collective-permute-start.2 = (bf16[128,2048]{1,0:T(8,128)(2,1)S(1)}, bf16[128,2048]{1,0:T(8,128)(2,1)S(1)}, u32[]{:S(2)}, u32[]{:S(2)}) collective-permute-start(bf16[128,2048]{1,0:T(8,128)(2,1)S(1)} %collective-permute-done.1), channel_id=1, source_target_pairs={{0,8},{8,16},{16,24},{24,0},{1,9},{9,17},{17,25},{25,1},{2,10},{10... | collective-permute-start | bytes 1572872 | tf_op jit(solution)/shard_map/ppermute | solution.py:108
  66.1 11.5 %copy-start.3 = (f32[512,512]{1,0:T(8,128)S(1)}, f32[512,512]{1,0:T(8,128)}, u32[]{:S(2)}) copy-start(f32[512,512]{1,0:T(8,128)} %fusion.11) | copy-start | bytes 3145732
  67.3 14.5 %copy-start.2 = (bf16[512,512]{0,1:T(8,128)(2,1)}, bf16[512,512]{0,1:T(8,128)(2,1)S(1)}, u32[]{:S(2)}) copy-start(bf16[512,512]{0,1:T(8,128)(2,1)S(1)} %copy.28) | copy-start | bytes 1572868
  69.7 1.7 %copy-start.4 = (bf16[512,4,32]{0,2,1:T(8,128)(2,1)}, bf16[512,4,32]{0,2,1:T(8,128)(2,1)S(1)}, u32[]{:S(2)}) copy-start(bf16[512,4,32]{0,2,1:T(8,128)(2,1)S(1)} %get-tuple-element.44) | copy-start | bytes 393220
Sparse Core Ops, SparseCore 0:
  9.8 49.5 all-gather.2
  61.0 80.8 all-gather.4
